TPU v7x, 32 devices: a whole 2x2x4 slice. The times are simulated.
32 devices in a mesh: grp: 2 (over y), ep: 4 (over z), tp: 4 (over x, core).
Axes of the slice: x: 2, y: 2, z: 4, core: 2. Of those that a mesh axis runs over, the one named last changes fastest.
Arguments:
- queries: bfloat16 [1024, 16, 128], P(('grp', 'ep'), 'tp'), parts along dimension 0, may hold values from -6 to 6
- key_vectors: bfloat16 [1024, 16, 128], P(('grp', 'ep'), 'tp'), parts along dimension 0, may hold values from -6 to 6
- values: bfloat16 [1024, 16, 128], P(('grp', 'ep'), 'tp'), parts along dimension 0, may hold values from -6 to 6
- forget_cum: float32 [1024, 16], P('grp', 'tp'), parts along dimension 0, may hold values from -90 to 0, as said below
- query_gain: float32 [128], replicated, may hold values from 0.1 to 5.5
- key_gain: float32 [128], replicated, may hold values from 0.1 to 5.5
- tokens: bfloat16 [4096, 4096], P(('grp', 'ep', 'tp')), parts along dimension 0, may hold values from -6 to 6
- norm_gain: float32 [4096], replicated, may hold values from 0.1 to 1.9
- routes: int32 [4096, 2], P(('grp', 'ep', 'tp')), parts along dimension 0, may hold values from 0 to 127, all different within a row; in each aligned block of 128 rows (0 to 127, 128 to 255, ...) at most 2 rows name the same one
- route_weights: float32 [4096, 2], P(('grp', 'ep', 'tp')), parts along dimension 0, may hold values from 0.3 to 1.2
- expert_gate: bfloat16 [128, 4096, 384], P(('ep', 'tp')), may hold values from -0.09375 to 0.09375
- expert_up: bfloat16 [128, 4096, 384], P(('ep', 'tp')), may hold values from -0.09375 to 0.09375
- expert_down: bfloat16 [128, 384, 4096], P(('ep', 'tp')), may hold values from -0.3125 to 0.3125
- shared_gate: bfloat16 [4096, 192], P(None, 'tp'), may hold values from -0.09375 to 0.09375
- shared_up: bfloat16 [4096, 192], P(None, 'tp'), may hold values from -0.09375 to 0.09375
- shared_down: bfloat16 [192, 4096], P('tp'), may hold values from -0.4375 to 0.4375
Outputs:
- attended: bfloat16 [1024, 16, 128], P(('grp', 'ep'), 'tp'), parts along dimension 0
- routed_output: bfloat16 [4096, 4096], P(('grp', 'ep', 'tp')), parts along dimension 0
There are 2 independent parts, one for each index of `grp`. A program takes and returns all parts, laid end to end along the dimension named above; an argument that names none is the same for every part. Nothing has to cross between parts.
Inputs may be any that keep to these rules, and one draw needn't show every extreme that they name: `routes`: each row names 2 different experts; the rows of one device name every expert exactly 2 times. `forget_cum`: never rises from one position to the next.
All inputs are finite; a program needn't handle non-finite values.
Results may differ from a plain program's by a relative error of at most 0.007.
The roundings to bfloat16 on the way count: a program that leaves them out, or rounds other values in their place, can miss the bound.
Values may be sent and summed in bfloat16 or wider, within the bound.
A program may use at most 128 MiB of HBM per device.

v0:
```python
import jax
import jax.numpy as jnp
from jax import lax
from jax.sharding import PartitionSpec as P

D = 4096
EXPERTS = 128
TOP_K = 2
CAP = 2


def rms_rows(row_values, gain_vector):
    widened = row_values.astype(jnp.float32)
    inverse = lax.rsqrt(jnp.mean(widened * widened, axis=-1, keepdims=True) + 1e-06)
    return (widened * inverse * gain_vector).astype(jnp.bfloat16)


def attend(queries, key_vectors, values, forget_cum, query_gain, key_gain):
    query_norm = rms_rows(queries, query_gain)
    key_norm = rms_rows(key_vectors, key_gain)
    query_rows = query_norm.shape[0]
    head_count = query_norm.shape[1]
    head_size = query_norm.shape[2]
    first_query = lax.axis_index("ep") * query_rows
    query_positions = first_query + lax.iota(jnp.int32, query_rows)
    last_query = first_query + query_rows - 1
    query_cum = lax.dynamic_slice_in_dim(forget_cum, first_query, query_rows, 0).T
    scale_factor = head_size ** (-0.5)
    start_state = (
        jnp.full((head_count, query_rows), -1e30, jnp.float32),
        jnp.zeros((head_count, query_rows), jnp.float32),
        jnp.zeros((head_count, query_rows, head_size), jnp.float32),
    )
    key_part = lax.all_gather(key_norm, "ep", axis=0, tiled=True)
    value_part = lax.all_gather(values, "ep", axis=0, tiled=True)
    piece_rows = key_part.shape[0]

    def compute(inner_state):
        best_score, denominator, accumulated = inner_state
        cum_block = forget_cum.T
        scores = jnp.einsum(
            "qhd,khd->hqk", query_norm, key_part, preferred_element_type=jnp.float32
        )
        scores = scores * scale_factor + query_cum[:, :, None] - cum_block[:, None, :]
        key_positions = lax.iota(jnp.int32, piece_rows)
        allowed = (key_positions[None, :] <= query_positions[:, None])[None]
        scores = jnp.where(allowed, scores, -1e30)
        new_best = jnp.maximum(best_score, jnp.max(scores, axis=2))
        weights = jnp.where(allowed, jnp.exp(scores - new_best[:, :, None]), 0.0)
        denominator = jnp.sum(weights, axis=2)
        product = jnp.einsum(
            "hqk,khd->hqd",
            weights.astype(jnp.bfloat16),
            value_part,
            preferred_element_type=jnp.float32,
        )
        accumulated = product
        return (new_best, denominator, accumulated)

    best_score, denominator, accumulated = lax.cond(
        jnp.int32(0) <= last_query, compute, lambda inner_state: inner_state, start_state
    )
    return (accumulated / denominator[:, :, None]).transpose(1, 0, 2).astype(jnp.bfloat16)


def shared_expert(normed, shared_gate, shared_up, shared_down):
    row_count = normed.shape[0]
    whole_gate, whole_up, whole_down = (
        lax.all_gather(shared_gate, "tp", axis=1, tiled=True),
        lax.all_gather(shared_up, "tp", axis=1, tiled=True),
        lax.all_gather(shared_down, "tp", axis=0, tiled=True),
    )
    block_total = lax.axis_size("tp")
    gate_values = jnp.dot(normed, whole_gate, preferred_element_type=jnp.float32)
    upward = jnp.dot(normed, whole_up, preferred_element_type=jnp.float32)
    hidden_whole = (jax.nn.silu(gate_values) * upward).astype(jnp.bfloat16)
    part_width = whole_down.shape[0] // block_total
    hidden_blocks = hidden_whole.reshape(row_count, block_total, part_width)
    down_blocks = whole_down.reshape(block_total, part_width, whole_down.shape[1])
    partials = jnp.einsum(
        "rnp,npd->nrd", hidden_blocks, down_blocks, preferred_element_type=jnp.float32
    ).astype(jnp.bfloat16)
    return jnp.sum(partials.astype(jnp.float32), axis=0).astype(jnp.bfloat16)


def mixture(
    tokens,
    norm_gain,
    routes,
    route_weights,
    expert_gate,
    expert_up,
    expert_down,
    shared_gate,
    shared_up,
    shared_down,
):
    normed = rms_rows(tokens, norm_gain)
    row_count = tokens.shape[0]
    shared_out = shared_expert(normed, shared_gate, shared_up, shared_down)
    flat_routes = routes.reshape(-1)
    choice_count = flat_routes.shape[0]
    one_hot = (flat_routes[:, None] == lax.iota(jnp.int32, EXPERTS)[None, :]).astype(jnp.int32)
    slot_rank = jnp.sum((jnp.cumsum(one_hot, axis=0) - one_hot) * one_hot, axis=1)
    slot_index = slot_rank * EXPERTS + flat_routes
    slot_ids = lax.iota(jnp.int32, CAP * EXPERTS)
    matches = slot_index[None, :] == slot_ids[:, None]
    source_row = jnp.sum(
        jnp.where(matches, lax.iota(jnp.int32, choice_count)[None, :] // TOP_K, 0), axis=1
    )
    filled = jnp.any(matches, axis=1)
    outgoing = jnp.where(filled[:, None], normed[source_row], jnp.zeros((), jnp.bfloat16)).reshape(
        CAP, EXPERTS, D
    )
    arrived = lax.all_to_all(outgoing, ("ep", "tp"), split_axis=1, concat_axis=1, tiled=True)
    local_count = expert_gate.shape[0]
    grouped = arrived.reshape(CAP, -1, local_count, D)
    gate_values = jnp.einsum(
        "csed,edf->csef", grouped, expert_gate, preferred_element_type=jnp.float32
    )
    upward = jnp.einsum("csed,edf->csef", grouped, expert_up, preferred_element_type=jnp.float32)
    hidden = (jax.nn.silu(gate_values) * upward).astype(jnp.bfloat16)
    produced = (
        jnp.einsum("csef,efd->csed", hidden, expert_down, preferred_element_type=jnp.float32)
        .astype(jnp.bfloat16)
        .reshape(CAP, -1, D)
    )
    returned = lax.all_to_all(produced, ("ep", "tp"), split_axis=1, concat_axis=1, tiled=True)
    picked_rows = returned.reshape(CAP * EXPERTS, D)[slot_index].reshape(row_count, TOP_K, D)
    routed = jnp.sum(route_weights[:, :, None] * picked_rows.astype(jnp.float32), axis=1)
    return (shared_out.astype(jnp.float32) + routed).astype(jnp.bfloat16)


def local(
    queries,
    key_vectors,
    values,
    forget_cum,
    query_gain,
    key_gain,
    tokens,
    norm_gain,
    routes,
    route_weights,
    expert_gate,
    expert_up,
    expert_down,
    shared_gate,
    shared_up,
    shared_down,
):
    attended = attend(queries, key_vectors, values, forget_cum, query_gain, key_gain)
    routed_output = mixture(
        tokens,
        norm_gain,
        routes,
        route_weights,
        expert_gate,
        expert_up,
        expert_down,
        shared_gate,
        shared_up,
        shared_down,
    )
    return (attended, routed_output)


def solution(mesh):
    placed = (
        P(("grp", "ep"), "tp", None),
        P(("grp", "ep"), "tp", None),
        P(("grp", "ep"), "tp", None),
        P("grp", "tp"),
        P(),
        P(),
        P(("grp", "ep", "tp"), None),
        P(),
        P(("grp", "ep", "tp"), None),
        P(("grp", "ep", "tp"), None),
        P(("ep", "tp"), None, None),
        P(("ep", "tp"), None, None),
        P(("ep", "tp"), None, None),
        P(None, "tp"),
        P(None, "tp"),
        P("tp", None),
    )
    return jax.shard_map(
        local,
        mesh=mesh,
        in_specs=placed,
        out_specs=(P(("grp", "ep"), "tp", None), P(("grp", "ep", "tp"), None)),
        check_vma=False,
    )
```

profile of v0, /device:TPU:0, one launch (start us, length us, event | category | flops | bytes accessed | tf_op | source)
XLA Modules:
  0.0 230.9 jit_solution(5048719747301511845)
XLA Ops:
  7.2 0.9 copy.80
  9.2 1.5 fusion.23
  10.9 0.3 fusion.25
  11.2 1.8 gather_fusion
  13.1 3.8 %broadcast_select_fusion = bf16[2,128,4096]{2,0,1:T(2,128)(2,1)} fusion(pred[2,128]{0,1:T(8,128)(4,1)S(1)} %copy.84, bf16[2,128,4096]{2,1,0:T(8,128)(2,1)S(1)} %bitcast.86), kind=kLoop, calls=%fused_computation.27 | loop fusion | flops 1048576 | bytes 4194560 | tf_op jit(solution)/shard_map/jit(_where)/select_n | solution.py:112
  16.9 7.4 %all-to-all-start = ((bf16[2,128,4096]{2,0,1:T(2,128)(2,1)}), bf16[2,128,4096]{2,0,1:T(2,128)(2,1)}, u32[]{:S(2)}, u32[]{:S(2)}) async-start(bf16[2,128,4096]{2,0,1:T(2,128)(2,1)} %broadcast_select_fusion), calls=%async_computation | async-start | bytes 4194304 | tf_op jit(solution)/shard_map/all_to_all | solution.py:115
  24.4 0.7 all-gather.4.cloned.1.call-update
  25.3 0.5 all-gather.6.cloned.1.call-update
  25.9 39.6 %all-to-all-done = bf16[2,128,4096]{2,0,1:T(2,128)(2,1)} async-done(((bf16[2,128,4096]{2,0,1:T(2,128)(2,1)}), bf16[2,128,4096]{2,0,1:T(2,128)(2,1)}, u32[]{:S(2)}, u32[]{:S(2)}) %all-to-all-start) | async-done | bytes 2097184 | tf_op jit(solution)/shard_map/all_to_all | solution.py:115
  65.5 2.9 %copy.120 = bf16[2,128,4096]{2,1,0:T(8,128)(2,1)S(1)} copy(bf16[2,128,4096]{2,0,1:T(2,128)(2,1)} %all-to-all-done) | data formatting | bytes 4194304 | tf_op jit(solution)/shard_map/all_to_all | solution.py:115
  68.4 10.7 %fusion.29 = f32[2,16,8,384]{3,1,0,2:T(8,128)S(1)} fusion(bf16[8,4096,384]{2,1,0:T(8,128)(2,1)} %param.28, bf16[2,16,8,4096]{3,2,1,0:T(8,128)(2,1)S(1)} %bitcast.84), kind=kOutput, calls=%fused_computation.39 | convolution fusion | flops 805306368 | bytes 27656192 | tf_op jit(solution)/shard_map/csed,edf->csef/dot_general | solution.py:118
  79.1 21.4 %fusion.20 = bf16[2,16,8,4096]{3,1,0,2:T(8,128)(2,1)} fusion(bf16[8,384,4096]{2,1,0:T(8,128)(2,1)} %param.30, bf16[8,4096,384]{2,1,0:T(8,128)(2,1)} %param.29, bf16[2,16,8,4096]{3,2,1,0:T(8,128)(2,1)S(1)} %bitcast.85, f32[2,16,8,384]{3,1,0,2:T(8,128)S(1)} %fusion.29), kind=kOutput, calls=%fused_computation.25 | convolution fusion | flops 1612251136 | bytes 54919168 | tf_op jit(solution)/shard_map/csef,efd->csed/dot_general | solution.py:124
  100.5 2.7 %copy.119 = bf16[2,16,8,4096]{3,2,1,0:T(8,128)(2,1)S(1)} copy(bf16[2,16,8,4096]{3,1,0,2:T(8,128)(2,1)} %fusion.20) | data formatting | bytes 4194304 | tf_op jit(solution)/shard_map/convert_element_type | solution.py:125
  103.3 3.5 %copy.90 = bf16[2,128,4096]{2,0,1:T(2,128)(2,1)} copy(bf16[2,128,4096]{2,1,0:T(8,128)(2,1)S(1)} %bitcast.87) | data formatting | bytes 4194304 | tf_op jit(solution)/shard_map/reshape | solution.py:126
  106.8 11.5 %all-to-all-start.1 = ((bf16[2,128,4096]{2,0,1:T(2,128)(2,1)}), bf16[2,128,4096]{2,0,1:T(2,128)(2,1)}, u32[]{:S(2)}, u32[]{:S(2)}) async-start(bf16[2,128,4096]{2,0,1:T(2,128)(2,1)} %copy.90), calls=%async_computation.1 | async-start | bytes 4194304 | tf_op jit(solution)/shard_map/all_to_all | solution.py:128
  118.3 0.3 all-gather.8.cloned.1.call-start
  118.5 0.5 all-gather.8.cloned.1.call-update
  119.8 57.6 %all_gather.15 = bf16[512,4,128]{2,0,1:T(8,128)(2,1)S(1)} all-gather(bf16[128,4,128]{2,0,1:T(8,128)(2,1)S(1)} %fusion.64), channel_id=1, replica_groups=mesh['grp'=2,'ep'=4,'tp'=4] {'ep'}, dimensions={0}, use_global_device_ids=true | all-gather | bytes 655360 | tf_op jit(solution)/shard_map/all_gather | solution.py:34
  177.5 15.9 %all_gather.16 = bf16[512,4,128]{2,0,1:T(8,128)(2,1)S(1)} all-gather(bf16[128,4,128]{2,0,1:T(8,128)(2,1)S(1)} %copy.76), channel_id=1, replica_groups=mesh['grp'=2,'ep'=4,'tp'=4] {'ep'}, dimensions={0}, use_global_device_ids=true | all-gather | bytes 655360 | tf_op jit(solution)/shard_map/all_gather | solution.py:35
  193.5 1.5 conditional.1
  193.6 0.5 fusion.75
  194.1 0.4 fusion.5
  194.7 0.3 fusion.4
  195.2 0.9 fusion.71
  196.0 2.0 fusion.76
  198.0 2.0 fusion.53
  200.1 2.8 %fusion.28 = bf16[128,4096]{1,0:T(8,128)(2,1)S(1)} fusion(bf16[128,4,48]{0,2,1:T(8,128)(2,1)S(1)} %bitcast.90, bf16[4,48,4096]{2,1,0:T(8,128)(2,1)} %bitcast.98), kind=kOutput, calls=%fused_computation.38 | convolution fusion | flops 204996608 | bytes 2670592 | tf_op jit(solution)/shard_map/rnp,npd->nrd/dot_general | solution.py:80
  202.9 2.9 %copy.91 = bf16[2,128,4096]{2,1,0:T(8,128)(2,1)S(1)} copy(bf16[2,128,4096]{2,0,1:T(2,128)(2,1)} %all-to-all-done.1) | data formatting | bytes 4194304 | tf_op jit(solution)/shard_map/all_to_all | solution.py:128
  205.8 3.2 %gather_fusion.1 = bf16[256,4096]{1,0:T(8,128)(2,1)} fusion(bf16[256,4096]{1,0:T(8,128)(2,1)S(1)} %bitcast.83, s32[1024]{0:T(1024)S(1)} %pad_clamp_fusion), kind=kCustom, calls=%fused_computation.1 | custom fusion | bytes 4195328 | tf_op jit(solution)/shard_map/gather | solution.py:129
  209.0 5.4 %reshape.195 = f32[128,2,4096]{2,1,0:T(2,128)} reshape(bf16[256,4096]{1,0:T(8,128)(2,1)} %gather_fusion.1) | data formatting | bytes 6291456 | tf_op jit(solution)/shard_map/convert_element_type | solution.py:130
  214.4 8.7 %multiply_reduce_fusion = f32[128,4096]{1,0:T(8,128)S(1)} fusion(f32[128,2,4096]{2,1,0:T(2,128)} %reshape.195, f32[128,2]{1,0:T(8,128)S(1)} %copy.79), kind=kLoop, calls=%fused_computation.26 | loop fusion | flops 1572864 | bytes 6292480 | tf_op jit(solution)/shard_map/reduce_sum | solution.py:130
  223.2 1.2 add_convert_fusion
  (64 shorter events, 2.9 us)
Async XLA Ops:
  7.2 3.7 %copy-start = (bf16[128,4096]{1,0:T(8,128)(2,1)S(1)}, bf16[128,4096]{1,0:T(8,128)(2,1)}, u32[]{:S(2)}) copy-start(bf16[128,4096]{1,0:T(8,128)(2,1)} %param.24) | copy-start | bytes 3145732
  7.2 3.7 %copy-start.6 = (f32[4096]{0:T(1024)S(1)}, f32[4096]{0:T(1024)}, u32[]{:S(2)}) copy-start(f32[4096]{0:T(1024)} %param.25) | copy-start | bytes 49156
  8.1 2.7 %copy-start.1 = (s32[128,2]{1,0:T(8,128)}, s32[128,2]{1,0:T(8,128)S(1)}, u32[]{:S(2)}) copy-start(s32[128,2]{1,0:T(8,128)S(1)} %copy.80) | copy-start | bytes 3076
  16.9 48.5 %all-to-all-start = ((bf16[2,128,4096]{2,0,1:T(2,128)(2,1)}), bf16[2,128,4096]{2,0,1:T(2,128)(2,1)}, u32[]{:S(2)}, u32[]{:S(2)}) async-start(bf16[2,128,4096]{2,0,1:T(2,128)(2,1)} %broadcast_select_fusion), calls=%async_computation | async-start | bytes 4194304 | tf_op jit(solution)/shard_map/all_to_all | solution.py:115
  24.4 171.6 %all-gather.4.cloned.1.call-start = ((), (), s32[]{:S(2)}) async-start(), calls=%async_computation.2 | async-start | bytes 1966080 | tf_op jit(solution)/shard_map/all_gather | solution.py:69
  25.1 172.9 %all-gather.6.cloned.1.call-start = ((), (), s32[]{:S(2)}) async-start(), calls=%async_computation.3 | async-start | bytes 1966080 | tf_op jit(solution)/shard_map/all_gather | solution.py:70
  106.8 12.3 %copy-start.2 = (s32[128,2]{1,0:T(8,128)S(1)}, s32[128,2]{1,0:T(8,128)}, u32[]{:S(2)}) copy-start(s32[128,2]{1,0:T(8,128)} %copy-done.1) | copy-start | bytes 3076
  106.8 12.4 %copy-start.7 = (f32[128,2]{0,1:T(2,128)S(1)}, f32[128,2]{0,1:T(2,128)}, u32[]{:S(2)}) copy-start(f32[128,2]{0,1:T(2,128)} %param.27) | copy-start | bytes 3076
  106.8 12.5 %copy-start.5 = (bf16[128,4,128]{2,1,0:T(4,128)(2,1)S(1)}, bf16[128,4,128]{2,1,0:T(4,128)(2,1)}, u32[]{:S(2)}) copy-start(bf16[128,4,128]{2,1,0:T(4,128)(2,1)} %param.20) | copy-start | bytes 393220
  106.8 12.6 %copy-start.10 = (f32[512,4]{0,1:T(4,128)S(1)}, f32[512,4]{0,1:T(4,128)}, u32[]{:S(2)}) copy-start(f32[512,4]{0,1:T(4,128)} %param.21) | copy-start | bytes 24580
  106.8 12.6 %copy-start.3 = (bf16[128,4,128]{2,1,0:T(4,128)(2,1)S(1)}, bf16[128,4,128]{2,1,0:T(4,128)(2,1)}, u32[]{:S(2)}) copy-start(bf16[128,4,128]{2,1,0:T(4,128)(2,1)} %param.19) | copy-start | bytes 393220
  106.8 12.7 %copy-start.4 = (bf16[128,4,128]{2,1,0:T(4,128)(2,1)S(1)}, bf16[128,4,128]{2,1,0:T(4,128)(2,1)}, u32[]{:S(2)}) copy-start(bf16[128,4,128]{2,1,0:T(4,128)(2,1)} %param.18) | copy-start | bytes 393220
  106.8 12.9 %copy-start.8 = (f32[128]{0:T(128)S(1)}, f32[128]{0:T(128)}, u32[]{:S(2)}) copy-start(f32[128]{0:T(128)} %param.23) | copy-start | bytes 1540
  106.8 96.0 %all-to-all-start.1 = ((bf16[2,128,4096]{2,0,1:T(2,128)(2,1)}), bf16[2,128,4096]{2,0,1:T(2,128)(2,1)}, u32[]{:S(2)}, u32[]{:S(2)}) async-start(bf16[2,128,4096]{2,0,1:T(2,128)(2,1)} %copy.90), calls=%async_computation.1 | async-start | bytes 4194304 | tf_op jit(solution)/shard_map/all_to_all | solution.py:128
  118.3 75.1 %copy-start.9 = (f32[128]{0:T(128)S(1)}, f32[128]{0:T(128)}, u32[]{:S(2)}) copy-start(f32[128]{0:T(128)} %param.22) | copy-start | bytes 1540
  118.3 81.8 %all-gather.8.cloned.1.call-start = ((), (), s32[]{:S(2)}) async-start(), calls=%async_computation.4 | async-start | bytes 1966080 | tf_op jit(solution)/shard_map/all_gather | solution.py:71
Sparse Core Ops, SparseCore 0:
  26.8 28.5 all-gather.3
  56.9 20.2 all-gather.5
  120.6 28.3 all-gather.7
where the time goes:
time: 231 us
  blocking collectives  73.5 us (32%)
  waiting for transfers between devices  41.3 us (18%)
  matrix products  39.7 us (17%)
  local copies, waits for them, and re-layouts  24.6 us (11%)
  starting transfers between devices  19.4 us (8%)
  other arithmetic  18.3 us (8%)
  between operations  14.1 us (6%)
    all_gather x1, blocking collectives, attend(): key_part = lax.all_gather(key_norm, 'ep', axis=0, tiled=True)  57.6 us
    all_to_all x1, waiting for transfers between devices, mixture(): lax.all_to_all(outgoing, ('ep', 'tp'), split_axis=1, concat_axis=1, tiled...  39.6 us
    dot_general x1, matrix products, mixture(): jnp.einsum('csef,efd->csed', hidden, expert_down, preferred_element_type=...  21.4 us
    all_gather x1, blocking collectives, attend(): value_part = lax.all_gather(values, 'ep', axis=0, tiled=True)  15.9 us
    all_to_all x1, starting transfers between devices, mixture(): lax.all_to_all(produced, ('ep', 'tp'), split_axis=1, concat_axis=1, tiled...  11.5 us
    dot_general x1, matrix products, mixture(): jnp.einsum('csed,edf->csef', grouped, expert_gate, preferred_element_type...  10.7 us
    reduce_sum x1, other arithmetic, mixture(): jnp.sum(route_weights[:, :, None] * picked_rows.astype(jnp.float32), axis=1)  8.75 us
    all_to_all x1, starting transfers between devices, mixture(): lax.all_to_all(outgoing, ('ep', 'tp'), split_axis=1, concat_axis=1, tiled...  7.44 us
  transfers between devices with their start and end apart: 5, of which 1 were waited for; matrix products, arithmetic and copies ran while one was open for 22% of the time, Pallas kernels for 0%

commit v1 on v0

--- a/solution.py
+++ b/solution.py
@@ -125,7 +125,12 @@
         .astype(jnp.bfloat16)
         .reshape(CAP, -1, D)
     )
-    returned = lax.all_to_all(produced, ("ep", "tp"), split_axis=1, concat_axis=1, tiled=True)
+    returned = jnp.concatenate(
+        lax.all_to_all(
+            jnp.stack(jnp.split(produced, lax.axis_size(("ep", "tp")), axis=1)), ("ep", "tp"), 0, 0
+        ),
+        axis=1,
+    )
     picked_rows = returned.reshape(CAP * EXPERTS, D)[slot_index].reshape(row_count, TOP_K, D)
     routed = jnp.sum(route_weights[:, :, None] * picked_rows.astype(jnp.float32), axis=1)
     return (shared_out.astype(jnp.float32) + routed).astype(jnp.bfloat16)

time: 231 us -> 240 us (1.039)
  local copies, waits for them, and re-layouts: 24.6 us -> 34 us
    unnamed x26 -> x39, local copies, waits for them, and re-layouts: 1.06 us -> 13.8 us
    all_to_all x1 -> x0, local copies, waits for them, and re-layouts: 2.92 us -> none  [mixture(): lax.all_to_all(produced, ('ep', 'tp'), split_axis=1, concat_axis=1, tiled...]
  transfers between devices with their start and end apart: 5 -> 5, of which waited for: 1 -> 1; matrix products, arithmetic and copies ran while one was open for 22% -> 26% of each run, Pallas kernels for 0% -> 0%
where the time goes in v1:
time: 240 us
  blocking collectives  71.6 us (30%)
  waiting for transfers between devices  41.5 us (17%)
  matrix products  40.4 us (17%)
  local copies, waits for them, and re-layouts  34 us (14%)
  starting transfers between devices  19.1 us (8%)
  other arithmetic  18.9 us (8%)
  between operations  14 us (6%)
    all_gather x1, blocking collectives, attend(): key_part = lax.all_gather(key_norm, 'ep', axis=0, tiled=True)  55.5 us
    all_to_all x1, waiting for transfers between devices, mixture(): lax.all_to_all(outgoing, ('ep', 'tp'), split_axis=1, concat_axis=1, tiled...  39.6 us
    dot_general x1, matrix products, mixture(): jnp.einsum('csef,efd->csed', hidden, expert_down, preferred_element_type=...  21.4 us
    all_gather x1, blocking collectives, attend(): value_part = lax.all_gather(values, 'ep', axis=0, tiled=True)  16.1 us
    unnamed x39, local copies, waits for them, and re-layouts  13.8 us
    all_to_all x1, starting transfers between devices, mixture(): lax.all_to_all(jnp.stack(jnp.split(produced, lax.axis_size(('ep', 'tp')),...  11.4 us
    dot_general x1, matrix products, mixture(): jnp.einsum('csed,edf->csef', grouped, expert_gate, preferred_element_type...  10.7 us
    reduce_sum x1, other arithmetic, mixture(): jnp.sum(route_weights[:, :, None] * picked_rows.astype(jnp.float32), axis=1)  8.75 us
  transfers between devices with their start and end apart: 5, of which 1 were waited for; matrix products, arithmetic and copies ran while one was open for 26% of the time, Pallas kernels for 0%

profile of v1, /device:TPU:0, one launch (start us, length us, event | category | flops | bytes accessed | tf_op | source)
XLA Modules:
  0.0 239.7 jit_solution(6207425893383146032)
XLA Ops:
  7.2 0.9 copy.94
  9.2 1.5 fusion.23
  11.2 1.8 gather_fusion
  13.1 3.8 %broadcast_select_fusion = bf16[2,128,4096]{2,0,1:T(2,128)(2,1)} fusion(pred[2,128]{0,1:T(8,128)(4,1)S(1)} %copy.98, bf16[2,128,4096]{2,1,0:T(8,128)(2,1)S(1)} %bitcast.167), kind=kLoop, calls=%fused_computation.27 | loop fusion | flops 1048576 | bytes 4194560 | tf_op jit(solution)/shard_map/jit(_where)/select_n | solution.py:112
  16.9 7.4 %all-to-all-start = ((bf16[2,128,4096]{2,0,1:T(2,128)(2,1)}), bf16[2,128,4096]{2,0,1:T(2,128)(2,1)}, u32[]{:S(2)}, u32[]{:S(2)}) async-start(bf16[2,128,4096]{2,0,1:T(2,128)(2,1)} %broadcast_select_fusion), calls=%async_computation | async-start | bytes 4194304 | tf_op jit(solution)/shard_map/all_to_all | solution.py:115
  24.4 0.7 all-gather.4.cloned.1.call-update
  25.9 39.6 %all-to-all-done = bf16[2,128,4096]{2,0,1:T(2,128)(2,1)} async-done(((bf16[2,128,4096]{2,0,1:T(2,128)(2,1)}), bf16[2,128,4096]{2,0,1:T(2,128)(2,1)}, u32[]{:S(2)}, u32[]{:S(2)}) %all-to-all-start) | async-done | bytes 2097184 | tf_op jit(solution)/shard_map/all_to_all | solution.py:115
  65.5 2.9 %copy.133 = bf16[2,128,4096]{2,1,0:T(8,128)(2,1)S(1)} copy(bf16[2,128,4096]{2,0,1:T(2,128)(2,1)} %all-to-all-done) | data formatting | bytes 4194304 | tf_op jit(solution)/shard_map/all_to_all | solution.py:115
  68.4 10.7 %fusion.29 = f32[2,16,8,384]{3,1,0,2:T(8,128)S(1)} fusion(bf16[8,4096,384]{2,1,0:T(8,128)(2,1)} %param.28, bf16[2,16,8,4096]{3,2,1,0:T(8,128)(2,1)S(1)} %bitcast.149), kind=kOutput, calls=%fused_computation.39 | convolution fusion | flops 805306368 | bytes 27656192 | tf_op jit(solution)/shard_map/csed,edf->csef/dot_general | solution.py:118
  79.1 21.4 %fusion.20 = bf16[2,16,8,4096]{3,1,0,2:T(8,128)(2,1)} fusion(bf16[8,384,4096]{2,1,0:T(8,128)(2,1)} %param.30, bf16[8,4096,384]{2,1,0:T(8,128)(2,1)} %param.29, bf16[2,16,8,4096]{3,2,1,0:T(8,128)(2,1)S(1)} %bitcast.150, f32[2,16,8,384]{3,1,0,2:T(8,128)S(1)} %fusion.29), kind=kOutput, calls=%fused_computation.25 | convolution fusion | flops 1612251136 | bytes 54919168 | tf_op jit(solution)/shard_map/csef,efd->csed/dot_general | solution.py:124
  100.5 2.7 %copy.132 = bf16[2,16,8,4096]{3,2,1,0:T(8,128)(2,1)S(1)} copy(bf16[2,16,8,4096]{3,1,0,2:T(8,128)(2,1)} %fusion.20) | data formatting | bytes 4194304 | tf_op jit(solution)/shard_map/convert_element_type | solution.py:125
  107.9 0.7 fusion.76
  113.8 11.4 %all-to-all-start.1 = ((bf16[16,2,8,4096]{3,2,1,0:T(8,128)(2,1)}), bf16[16,2,8,4096]{3,2,1,0:T(8,128)(2,1)S(1)}, u32[]{:S(2)}, u32[]{:S(2)}) async-start(bf16[16,2,8,4096]{3,2,1,0:T(8,128)(2,1)} %fusion.68), calls=%async_computation.1 | async-start | bytes 4194304 | tf_op jit(solution)/shard_map/all_to_all | solution.py:129
  125.3 0.7 all-gather.8.cloned.1.call-update
  126.1 0.7 copy.93
  126.9 0.9 copy.90
  127.8 0.7 dynamic-slice_bitcast_fusion
  128.9 55.5 %all_gather.15 = bf16[512,4,128]{2,0,1:T(8,128)(2,1)S(1)} all-gather(bf16[128,4,128]{2,0,1:T(8,128)(2,1)S(1)} %fusion.64), channel_id=1, replica_groups=mesh['grp'=2,'ep'=4,'tp'=4] {'ep'}, dimensions={0}, use_global_device_ids=true | all-gather | bytes 655360 | tf_op jit(solution)/shard_map/all_gather | solution.py:34
  184.5 16.1 %all_gather.16 = bf16[512,4,128]{2,0,1:T(8,128)(2,1)S(1)} all-gather(bf16[128,4,128]{2,0,1:T(8,128)(2,1)S(1)} %copy.90), channel_id=1, replica_groups=mesh['grp'=2,'ep'=4,'tp'=4] {'ep'}, dimensions={0}, use_global_device_ids=true | all-gather | bytes 655360 | tf_op jit(solution)/shard_map/all_gather | solution.py:35
  200.6 0.8 fusion.61
  201.4 2.2 conditional.1
  201.5 1.2 fusion.91
  203.7 0.9 fusion.87
  204.6 2.0 fusion.92
  206.6 2.0 fusion.53
  208.6 2.8 %fusion.28 = bf16[128,4096]{1,0:T(8,128)(2,1)S(1)} fusion(bf16[128,4,48]{0,2,1:T(8,128)(2,1)S(1)} %bitcast.171, bf16[4,48,4096]{2,1,0:T(8,128)(2,1)} %bitcast.179), kind=kOutput, calls=%fused_computation.38 | convolution fusion | flops 204996608 | bytes 2670592 | tf_op jit(solution)/shard_map/rnp,npd->nrd/dot_general | solution.py:80
  211.5 1.3 copy-done
  212.8 1.7 copy.104
  214.5 3.2 %gather_fusion.1 = bf16[256,4096]{1,0:T(8,128)(2,1)} fusion(bf16[256,4096]{1,0:T(8,128)(2,1)S(1)} %bitcast.148, s32[1024]{0:T(1024)S(1)} %pad_clamp_fusion), kind=kCustom, calls=%fused_computation.1 | custom fusion | bytes 4195328 | tf_op jit(solution)/shard_map/gather | solution.py:134
  217.7 5.5 %reshape.195 = f32[128,2,4096]{2,1,0:T(2,128)} reshape(bf16[256,4096]{1,0:T(8,128)(2,1)} %gather_fusion.1) | data formatting | bytes 6291456 | tf_op jit(solution)/shard_map/convert_element_type | solution.py:135
  223.2 8.7 %multiply_reduce_fusion = f32[128,4096]{1,0:T(8,128)S(1)} fusion(f32[128,2,4096]{2,1,0:T(2,128)} %reshape.195, f32[128,2]{1,0:T(8,128)S(1)} %copy-done.6), kind=kLoop, calls=%fused_computation.26 | loop fusion | flops 1572864 | bytes 6292480 | tf_op jit(solution)/shard_map/reduce_sum | solution.py:135
  231.9 1.2 add_convert_fusion
  (77 shorter events, 14.0 us)
Async XLA Ops:
  7.2 3.7 %copy-start.1 = (bf16[128,4096]{1,0:T(8,128)(2,1)S(1)}, bf16[128,4096]{1,0:T(8,128)(2,1)}, u32[]{:S(2)}) copy-start(bf16[128,4096]{1,0:T(8,128)(2,1)} %param.24) | copy-start | bytes 3145732
  7.2 3.7 %copy-start.7 = (f32[4096]{0:T(1024)S(1)}, f32[4096]{0:T(1024)}, u32[]{:S(2)}) copy-start(f32[4096]{0:T(1024)} %param.25) | copy-start | bytes 49156
  8.1 2.7 %copy-start.2 = (s32[128,2]{1,0:T(8,128)}, s32[128,2]{1,0:T(8,128)S(1)}, u32[]{:S(2)}) copy-start(s32[128,2]{1,0:T(8,128)S(1)} %copy.94) | copy-start | bytes 3076
  16.9 48.5 %all-to-all-start = ((bf16[2,128,4096]{2,0,1:T(2,128)(2,1)}), bf16[2,128,4096]{2,0,1:T(2,128)(2,1)}, u32[]{:S(2)}, u32[]{:S(2)}) async-start(bf16[2,128,4096]{2,0,1:T(2,128)(2,1)} %broadcast_select_fusion), calls=%async_computation | async-start | bytes 4194304 | tf_op jit(solution)/shard_map/all_to_all | solution.py:115
  24.4 180.2 %all-gather.4.cloned.1.call-start = ((), (), s32[]{:S(2)}) async-start(), calls=%async_computation.2 | async-start | bytes 1966080 | tf_op jit(solution)/shard_map/all_gather | solution.py:69
  25.1 181.5 %all-gather.6.cloned.1.call-start = ((), (), s32[]{:S(2)}) async-start(), calls=%async_computation.3 | async-start | bytes 1966080 | tf_op jit(solution)/shard_map/all_gather | solution.py:70
  113.8 12.2 %copy-start.3 = (s32[128,2]{1,0:T(8,128)S(1)}, s32[128,2]{1,0:T(8,128)}, u32[]{:S(2)}) copy-start(s32[128,2]{1,0:T(8,128)} %copy-done.2) | copy-start | bytes 3076
  113.8 12.3 %copy-start.8 = (f32[128,2]{0,1:T(2,128)S(1)}, f32[128,2]{0,1:T(2,128)}, u32[]{:S(2)}) copy-start(f32[128,2]{0,1:T(2,128)} %param.27) | copy-start | bytes 3076
  113.8 14.7 %copy-start.4 = (bf16[128,4,128]{2,1,0:T(4,128)(2,1)S(1)}, bf16[128,4,128]{2,1,0:T(4,128)(2,1)}, u32[]{:S(2)}) copy-start(bf16[128,4,128]{2,1,0:T(4,128)(2,1)} %param.19) | copy-start | bytes 393220
  113.8 14.8 %copy-start.5 = (bf16[128,4,128]{2,1,0:T(4,128)(2,1)S(1)}, bf16[128,4,128]{2,1,0:T(4,128)(2,1)}, u32[]{:S(2)}) copy-start(bf16[128,4,128]{2,1,0:T(4,128)(2,1)} %param.18) | copy-start | bytes 393220
  113.8 15.0 %copy-start.9 = (f32[128]{0:T(128)S(1)}, f32[128]{0:T(128)}, u32[]{:S(2)}) copy-start(f32[128]{0:T(128)} %param.23) | copy-start | bytes 1540
  113.8 97.6 %all-to-all-start.1 = ((bf16[16,2,8,4096]{3,2,1,0:T(8,128)(2,1)}), bf16[16,2,8,4096]{3,2,1,0:T(8,128)(2,1)S(1)}, u32[]{:S(2)}, u32[]{:S(2)}) async-start(bf16[16,2,8,4096]{3,2,1,0:T(8,128)(2,1)} %fusion.68), calls=%async_computation.1 | async-start | bytes 4194304 | tf_op jit(solution)/shard_map/all_to_all | solution.py:129
  125.2 83.4 %all-gather.8.cloned.1.call-start = ((), (), s32[]{:S(2)}) async-start(), calls=%async_computation.4 | async-start | bytes 1966080 | tf_op jit(solution)/shard_map/all_gather | solution.py:71
  211.4 1.4 copy-start
  217.7 5.5 %copy-start.6 = (f32[128,2]{1,0:T(8,128)S(1)}, f32[128,2]{1,0:T(8,128)}, u32[]{:S(2)}) copy-start(f32[128,2]{1,0:T(8,128)} %copy.93) | copy-start | bytes 3076
Sparse Core Ops, SparseCore 0:
  26.8 28.5 all-gather.3
  56.9 20.2 all-gather.5
  127.6 28.3 all-gather.7
